TPU v7x, 32 devices: a whole 2x2x4 slice. The times are simulated.
32 devices in a mesh: ep: 8 (over z, y), tp: 4 (over x, core).
Axes of the slice: x: 2, y: 2, z: 4, core: 2. Of those that a mesh axis runs over, the one named last changes fastest.
Arguments:
- residual_in: bfloat16 [16, 2048], P('ep'), may hold values from -6 to 6
- gla_state: float32 [16, 4, 256, 512], P('ep', 'tp'), may hold values from -6 to 6
- norm_gain: bfloat16 [2048], replicated, may hold values from 0.099609375 to 1.8984375
- w_query: bfloat16 [2048, 1024], P('ep', 'tp'), may hold values from -0.125 to 0.125
- w_key: bfloat16 [2048, 1024], P('ep', 'tp'), may hold values from -0.125 to 0.125
- w_value: bfloat16 [2048, 2048], P('ep', 'tp'), may hold values from -0.125 to 0.125
- w_decay: bfloat16 [2048, 1024], P('ep', 'tp'), may hold values from -0.5 to 0.5
- decay_bias: float32 [1024], P('tp'), may hold values from -40 to 8
- head_gain: bfloat16 [512], replicated, may hold values from 0.099609375 to 1.8984375
- w_output: bfloat16 [2048, 2048], P('tp', 'ep'), may hold values from -0.125 to 0.125
- ffn_gain: bfloat16 [2048], replicated, may hold values from 0.099609375 to 1.8984375
- router_group: bfloat16 [2048, 4], replicated, may hold values from -0.125 to 0.125
- router_expert: bfloat16 [8, 2048], replicated, may hold values from -0.125 to 0.125
- expert_ids: int32 [16, 2], replicated, may hold values from 0 to 7, all different within a row; in each aligned block of 16 rows (0 to 15, 16 to 31, ...) at most 16 rows name the same one
- w_gate: bfloat16 [8, 2048, 512], P('ep', None, 'tp'), may hold values from -0.125 to 0.125
- w_up: bfloat16 [8, 2048, 512], P('ep', None, 'tp'), may hold values from -0.125 to 0.125
- w_down: bfloat16 [8, 512, 2048], P('ep', 'tp'), may hold values from -0.75 to 0.75
Outputs:
- layer_out: bfloat16 [16, 2048], P('ep')
- new_state: float32 [16, 4, 256, 512], P('ep', 'tp')
Inputs may be any that keep to these rules, and one draw needn't show every extreme that they name: `expert_ids`: each row names 2 different experts; no expert is named by more than 16 rows of the whole batch, a bound that some block reaches.
All inputs are finite; a program needn't handle non-finite values.
Results may differ from a plain program's by a relative error of at most 0.023.
Values may be sent and summed in bfloat16 or wider, within the bound.
A program may use at most 64 MiB of HBM per device.

v0:
```python
import jax
import jax.numpy as jnp
from jax import lax
from jax.sharding import PartitionSpec as P

CAP = 16


EPSILON = 1e-06
GATE_SCALE = 16.0


def rms_scale(values, gain_vec):
    floats = values.astype(jnp.float32)
    return (
        floats
        * lax.rsqrt(jnp.mean(floats * floats, axis=-1, keepdims=True) + EPSILON)
        * gain_vec.astype(jnp.float32)
    )


def finish_part(hidden_res, moe_part, tp_index):
    part_cols = moe_part.shape[1]
    own_cols = lax.dynamic_slice_in_dim(hidden_res, tp_index * part_cols, part_cols, 1)
    return (own_cols.astype(jnp.float32) + moe_part).astype(jnp.bfloat16)


def on_device(
    residual_in,
    gla_state,
    norm_gain,
    w_query,
    w_key,
    w_value,
    w_decay,
    decay_bias,
    head_gain,
    w_output,
    ffn_gain,
    router_group,
    router_expert,
    expert_ids,
    w_gate,
    w_up,
    w_down,
):
    seq_rows = residual_in.shape[0]
    key_width = w_query.shape[1]
    value_width = w_value.shape[1]
    normed = rms_scale(residual_in, norm_gain).astype(jnp.bfloat16)
    columns = lax.all_to_all(normed, "ep", split_axis=1, concat_axis=0, tiled=True)
    projected = lax.psum_scatter(
        jnp.concatenate(
            [
                jnp.dot(columns, w_query, preferred_element_type=jnp.float32),
                jnp.dot(columns, w_key, preferred_element_type=jnp.float32),
                jnp.dot(columns, w_value, preferred_element_type=jnp.float32),
                jnp.dot(columns, w_decay, preferred_element_type=jnp.float32),
            ],
            axis=1,
        ),
        "ep",
        scatter_dimension=0,
        tiled=True,
    )
    query_rows = projected[:, :key_width].astype(jnp.bfloat16)
    key_rows = projected[:, key_width : 2 * key_width].astype(jnp.bfloat16)
    value_rows = projected[:, 2 * key_width : 2 * key_width + value_width].astype(jnp.bfloat16)
    decay_pre = projected[:, 2 * key_width + value_width :]
    log_decay = jax.nn.log_sigmoid(decay_pre + decay_bias) / GATE_SCALE
    query_float = lax.optimization_barrier(query_rows).astype(jnp.float32) * key_width ** (-0.5)
    key_float = lax.optimization_barrier(key_rows).astype(jnp.float32)
    value_float = lax.optimization_barrier(value_rows).astype(jnp.float32)
    old_state = gla_state[:, 0]
    new_state = (
        jnp.exp(log_decay)[:, :, None] * old_state + key_float[:, :, None] * value_float[:, None, :]
    )
    read_out = jnp.einsum("tk,tkv->tv", query_float, new_state, precision=lax.Precision.HIGHEST)
    gated_heads = rms_scale(read_out, head_gain).astype(jnp.bfloat16)
    partial_out = jnp.dot(
        lax.all_gather(gated_heads, "ep", axis=0, tiled=True),
        w_output,
        preferred_element_type=jnp.float32,
    ).astype(jnp.bfloat16)
    returned = lax.all_to_all(partial_out, "ep", split_axis=0, concat_axis=1, tiled=True)
    attention = lax.psum(returned.astype(jnp.float32).astype(jnp.bfloat16), "tp").astype(
        jnp.float32
    )
    hidden_res = (residual_in.astype(jnp.float32) + attention).astype(jnp.bfloat16)
    moe_in = rms_scale(hidden_res, ffn_gain).astype(jnp.bfloat16)
    expert = lax.axis_index("ep")
    is_named = jnp.any(expert_ids == expert, axis=1)
    slot_of = jnp.cumsum(is_named.astype(jnp.int32)) - 1
    slot_index = jnp.arange(CAP, dtype=jnp.int32)
    select_int = (is_named[None, :] & (slot_of[None, :] == slot_index[:, None])).astype(jnp.int32)
    select_bf = select_int.astype(jnp.bfloat16)
    slot_rows = jnp.dot(
        select_bf,
        lax.all_gather(moe_in, "ep", axis=0, tiled=True),
        preferred_element_type=jnp.float32,
    ).astype(jnp.bfloat16)
    slot_ids = jnp.sum(select_int[:, :, None] * expert_ids[None, :, :], axis=1)
    rival_ids = jnp.where(slot_ids[:, 0] == expert, slot_ids[:, 1], slot_ids[:, 0])
    group_logits = jnp.dot(slot_rows, router_group, preferred_element_type=jnp.float32)
    per_group = router_expert.shape[0] // router_group.shape[1]
    own_group = jnp.arange(router_group.shape[1], dtype=jnp.int32) == expert // per_group
    group_logit = jnp.sum(
        jnp.where(own_group[None, :], group_logits, jnp.zeros_like(group_logits)), axis=1
    )
    group_share = 1.0 / jnp.sum(jnp.exp(group_logits - group_logit[:, None]), axis=1)
    chosen = jnp.dot(slot_rows, router_expert[expert], preferred_element_type=jnp.float32)
    rival_logit = jnp.einsum(
        "cd,cd->c", slot_rows, router_expert[rival_ids], preferred_element_type=jnp.float32
    )
    slot_weight = group_share * jax.nn.sigmoid(chosen - rival_logit)
    gate_out = jnp.dot(slot_rows, w_gate[0], preferred_element_type=jnp.float32)
    up_out = jnp.dot(slot_rows, w_up[0], preferred_element_type=jnp.float32)
    hidden = (jax.nn.silu(gate_out) * up_out).astype(jnp.bfloat16)
    output = jnp.dot(hidden, w_down[0], preferred_element_type=jnp.float32)
    select_float = select_int.astype(jnp.float32)
    width_piece = lax.psum_scatter(
        output.astype(jnp.bfloat16), "tp", scatter_dimension=1, tiled=True
    ).astype(jnp.float32)
    weighted_piece = width_piece * slot_weight[:, None]
    piece_cols = weighted_piece.shape[1]
    outgoing = jnp.dot(select_float.T, weighted_piece, precision=lax.Precision.HIGHEST)
    owners = outgoing.shape[0] // seq_rows
    outgoing = outgoing.reshape(owners, seq_rows, piece_cols)
    arrived = lax.all_to_all(
        outgoing.astype(jnp.bfloat16), "ep", split_axis=0, concat_axis=0, tiled=True
    ).astype(outgoing.dtype)
    moe_piece = jnp.sum(arrived, axis=0)
    layer_piece = finish_part(hidden_res, moe_piece, lax.axis_index("tp"))
    layer_out = lax.all_gather(layer_piece, "tp", axis=1, tiled=True)
    return (layer_out, new_state[:, None])


def solution(mesh):
    placed = (
        P("ep", None),
        P("ep", "tp", None, None),
        P(),
        P("ep", "tp"),
        P("ep", "tp"),
        P("ep", "tp"),
        P("ep", "tp"),
        P("tp"),
        P(),
        P("tp", "ep"),
        P(),
        P(),
        P(),
        P(),
        P("ep", None, "tp"),
        P("ep", None, "tp"),
        P("ep", "tp", None),
    )
    return jax.shard_map(
        on_device,
        mesh=mesh,
        in_specs=placed,
        out_specs=(P("ep", None), P("ep", "tp", None, None)),
        check_vma=False,
    )
```

profile of v0, /device:TPU:0, one launch (start us, length us, event | category | flops | bytes accessed | tf_op | source)
XLA Modules:
  0.0 217.5 jit_solution(11208701178793737976)
XLA Ops:
  7.2 0.0 copy-start
  7.2 0.0 copy-start.12
  7.2 0.0 copy-start.8
  7.2 0.0 copy-start.6
  7.2 0.0 copy-start.2
  7.2 0.9 fusion.25
  8.2 0.0 copy-done.8
  8.2 1.4 fusion.27
  9.6 7.3 %all-to-all-start = ((bf16[2,8,256]{2,0,1:T(2,128)(2,1)}), bf16[2,8,256]{2,0,1:T(2,128)(2,1)S(1)}, u32[]{:S(2)}, u32[]{:S(2)}) async-start(bf16[2,8,256]{2,0,1:T(2,128)(2,1)} %bitcast), calls=%async_computation | async-start | bytes 16384 | tf_op jit(solution)/shard_map/all_to_all | solution.py:51
  16.9 0.0 all-reduce.3.cloned.1.call-start
  16.9 0.7 compare_reduce_fusion
  17.6 0.1 copy.30
  17.8 0.1 add_reduce_fusion
  17.9 0.8 multiply_reduce_fusion
  18.7 0.7 convert_element_type.109
  19.4 0.0 copy-done.12
  19.4 0.6 dynamic-slice
  20.6 2.8 %all-to-all-done = bf16[2,8,256]{2,0,1:T(2,128)(2,1)S(1)} async-done(((bf16[2,8,256]{2,0,1:T(2,128)(2,1)}), bf16[2,8,256]{2,0,1:T(2,128)(2,1)S(1)}, u32[]{:S(2)}, u32[]{:S(2)}) %all-to-all-start) | async-done | bytes 8224 | tf_op jit(solution)/shard_map/all_to_all | solution.py:51
  23.4 0.1 fusion.66
  23.6 1.1 fusion.64
  24.6 1.1 fusion.63
  25.7 1.1 fusion.65
  26.8 0.7 pad_maximum_fusion
  27.4 0.0 all-reduce.3.cloned.1.call-update
  27.5 68.3 %all-reduce.3.cloned.1.call-done = f32[16,1280]{1,0:T(8,128)} async-done(((f32[16,1280]{1,0:T(8,128)}), f32[16,1280]{1,0:T(8,128)}) %all-reduce.3.cloned.1.call-update) | async-done | bytes 81936
  95.7 0.8 dynamic-slice_convert_fusion
  96.6 0.0 copy-start.10
  96.6 0.7 copy-done.10
  97.2 0.8 fusion.54
  98.0 0.0 copy-done.2
  98.0 0.0 copy-start.5
  98.1 0.8 fusion.8
  98.8 0.1 fusion.44
  99.0 0.1 fusion.57
  99.0 26.1 %all-gather = bf16[8,2,512]{2,1,0:T(2,128)(2,1)S(1)} all-gather(bf16[1,2,512]{2,1,0:T(2,128)(2,1)S(1)} %fusion.57), channel_id=1, replica_groups=mesh['ep'=8,'tp'=4] {'ep'}, dimensions={0}, use_global_device_ids=true | all-gather | bytes 18432 | tf_op jit(solution)/shard_map/all_gather | solution.py:81
  125.2 0.1 convolution_convert_fusion.3
  125.3 0.6 all_to_all.35
  126.0 3.3 %all-to-all-start.1 = ((bf16[8,2,256]{2,1,0:T(2,128)(2,1)}), bf16[8,2,256]{2,1,0:T(2,128)(2,1)S(1)}, u32[]{:S(2)}, u32[]{:S(2)}) async-start(bf16[8,2,256]{2,1,0:T(2,128)(2,1)} %all_to_all.35), calls=%async_computation.1 | async-start | bytes 16384 | tf_op jit(solution)/shard_map/all_to_all | solution.py:85
  129.3 0.0 reduce-scatter.2.cloned.1.call-start
  129.4 0.0 copy-start.9
  129.4 0.7 copy-done.9
  130.1 0.6 gather_fusion
  130.7 5.1 %all-to-all-done.1 = bf16[8,2,256]{2,1,0:T(2,128)(2,1)S(1)} async-done(((bf16[8,2,256]{2,1,0:T(2,128)(2,1)}), bf16[8,2,256]{2,1,0:T(2,128)(2,1)S(1)}, u32[]{:S(2)}, u32[]{:S(2)}) %all-to-all-start.1) | async-done | bytes 8224 | tf_op jit(solution)/shard_map/all_to_all | solution.py:85
  135.8 5.9 %psum.7 = bf16[2,2048]{1,0:T(2,128)(2,1)S(1)} all-reduce(bf16[2,2048]{1,0:T(2,128)(2,1)S(1)} %bitcast.76), channel_id=1, replica_groups=mesh['ep'=8,'tp'=4] {'tp'}, use_global_device_ids=true, to_apply=%region_3.4 | all-reduce | flops 4096 | bytes 16384 | tf_op jit(solution)/shard_map/psum | solution.py:86
  141.6 0.0 copy-start.3
  141.7 0.1 fusion.22
  141.8 0.1 fusion.38
  141.9 30.5 %all-gather.1 = bf16[8,2,2048]{2,1,0:T(2,128)(2,1)S(1)} all-gather(bf16[1,2,2048]{2,1,0:T(2,128)(2,1)S(1)} %fusion.38), channel_id=1, replica_groups=mesh['ep'=8,'tp'=4] {'ep'}, dimensions={0}, use_global_device_ids=true | all-gather | bytes 73728 | tf_op jit(solution)/shard_map/all_gather | solution.py:99
  172.5 0.2 fusion.19
  172.7 0.2 fusion.14
  172.9 0.0 copy-done.3
  172.9 1.0 convolution_convert_fusion
  173.9 0.0 reduce-scatter.2.cloned.1.call-update
  173.9 0.7 copy-done.11
  174.6 0.1 select_reduce_fusion
  174.8 0.1 fusion.6
  174.9 16.2 %reduce-scatter.2.cloned.1.call-done = bf16[16,512]{1,0:T(8,128)(2,1)} async-done(((bf16[16,2048]{1,0:T(8,128)(2,1)}), bf16[16,512]{1,0:T(8,128)(2,1)}) %reduce-scatter.2.cloned.1.call-update) | async-done | bytes 16400 | tf_op jit(solution)/shard_map/reduce_scatter | solution.py:121
  191.2 0.9 convolution_convert_fusion.2
  192.1 0.6 convert_element_type.128
  192.7 5.5 %all-to-all-start.2 = ((bf16[8,2,512]{2,1,0:T(2,128)(2,1)}), bf16[8,2,512]{2,1,0:T(2,128)(2,1)S(1)}, u32[]{:S(2)}, u32[]{:S(2)}) async-start(bf16[8,2,512]{2,1,0:T(2,128)(2,1)} %convert_element_type.128), calls=%async_computation.3 | async-start | bytes 32768 | tf_op jit(solution)/shard_map/all_to_all | solution.py:129
  198.2 1.2 multiply_add_fusion
  199.4 5.4 %all-to-all-done.2 = bf16[8,2,512]{2,1,0:T(2,128)(2,1)S(1)} async-done(((bf16[8,2,512]{2,1,0:T(2,128)(2,1)}), bf16[8,2,512]{2,1,0:T(2,128)(2,1)S(1)}, u32[]{:S(2)}, u32[]{:S(2)}) %all-to-all-start.2) | async-done | bytes 16416 | tf_op jit(solution)/shard_map/all_to_all | solution.py:129
  204.9 5.2 %all_gather.11 = bf16[2,2048]{1,0:T(2,128)(2,1)S(1)} all-gather(bf16[2,512]{1,0:T(2,128)(2,1)S(1)} %add_convert_fusion), channel_id=1, replica_groups=mesh['ep'=8,'tp'=4] {'tp'}, dimensions={1}, use_global_device_ids=true | all-gather | bytes 10240 | tf_op jit(solution)/shard_map/all_gather | solution.py:134
  210.1 0.6 copy.46
  (32 shorter events, 0.3 us)
Async XLA Ops:
  7.2 165.7 %copy-start = (bf16[1,128,2048]{2,1,0:T(8,128)(2,1)S(1)}, bf16[1,128,2048]{2,1,0:T(8,128)(2,1)}, u32[]{:S(2)}) copy-start(bf16[1,128,2048]{2,1,0:T(8,128)(2,1)} %param.33) | copy-start | bytes 1572868
  7.2 12.2 %copy-start.12 = (u32[32]{0:T(128)S(1)}, u32[32]{0:T(128)}, u32[]{:S(2)}) copy-start(u32[32]{0:T(128)} %constant.70) | copy-start | bytes 388
  7.2 1.0 copy-start.8
  7.2 16.2 %copy-start.6 = (bf16[256,256]{1,0:T(8,128)(2,1)S(1)}, bf16[256,256]{1,0:T(8,128)(2,1)}, u32[]{:S(2)}) copy-start(bf16[256,256]{1,0:T(8,128)(2,1)} %param.23) | copy-start | bytes 393220
  7.2 90.8 %copy-start.2 = (f32[2,1,256,512]{3,2,1,0:T(8,128)S(1)}, f32[2,1,256,512]{3,2,1,0:T(8,128)}, u32[]{:S(2)}) copy-start(f32[2,1,256,512]{3,2,1,0:T(8,128)} %param.18) | copy-start | bytes 3145732
  9.6 13.8 %all-to-all-start = ((bf16[2,8,256]{2,0,1:T(2,128)(2,1)}), bf16[2,8,256]{2,0,1:T(2,128)(2,1)S(1)}, u32[]{:S(2)}, u32[]{:S(2)}) async-start(bf16[2,8,256]{2,0,1:T(2,128)(2,1)} %bitcast), calls=%async_computation | async-start | bytes 16384 | tf_op jit(solution)/shard_map/all_to_all | solution.py:51
  16.9 78.8 %all-reduce.3.cloned.1.call-start = ((), (), s32[]{:S(2)}) async-start(), calls=%async_computation.5 | async-start | bytes 163840
  96.6 0.7 copy-start.10
  98.0 27.1 %copy-start.5 = (bf16[512,256]{1,0:T(8,128)(2,1)S(1)}, bf16[512,256]{1,0:T(8,128)(2,1)}, u32[]{:S(2)}) copy-start(bf16[512,256]{1,0:T(8,128)(2,1)} %param.26) | copy-start | bytes 786436
  125.3 4.7 %copy-start.1 = (bf16[8,2048]{1,0:T(8,128)(2,1)S(1)}, bf16[8,2048]{1,0:T(8,128)(2,1)}, u32[]{:S(2)}) copy-start(bf16[8,2048]{1,0:T(8,128)(2,1)} %param.29) | copy-start | bytes 98308
  126.0 9.8 %all-to-all-start.1 = ((bf16[8,2,256]{2,1,0:T(2,128)(2,1)}), bf16[8,2,256]{2,1,0:T(2,128)(2,1)S(1)}, u32[]{:S(2)}, u32[]{:S(2)}) async-start(bf16[8,2,256]{2,1,0:T(2,128)(2,1)} %all_to_all.35), calls=%async_computation.1 | async-start | bytes 16384 | tf_op jit(solution)/shard_map/all_to_all | solution.py:85
  129.3 61.9 %reduce-scatter.2.cloned.1.call-start = ((), (), s32[]{:S(2)}) async-start(), calls=%async_computation.4 | async-start | bytes 81920 | tf_op jit(solution)/shard_map/reduce_scatter | solution.py:121
  129.4 0.7 copy-start.9
  130.1 42.6 %copy-start.4 = (bf16[1,2048,128]{2,1,0:T(8,128)(2,1)S(1)}, bf16[1,2048,128]{2,1,0:T(8,128)(2,1)}, u32[]{:S(2)}) copy-start(bf16[1,2048,128]{2,1,0:T(8,128)(2,1)} %param.31) | copy-start | bytes 1572868
  135.8 5.9 %copy-start.7 = (bf16[2,2048]{1,0:T(2,128)(2,1)S(1)}, bf16[2,2048]{1,0:T(2,128)(2,1)}, u32[]{:S(2)}) copy-start(bf16[2,2048]{1,0:T(2,128)(2,1)} %param.17) | copy-start | bytes 24580
  141.6 31.3 %copy-start.3 = (bf16[1,2048,128]{2,1,0:T(8,128)(2,1)S(1)}, bf16[1,2048,128]{2,1,0:T(8,128)(2,1)}, u32[]{:S(2)}) copy-start(bf16[1,2048,128]{2,1,0:T(8,128)(2,1)} %param.32) | copy-start | bytes 1572868
  173.9 0.7 copy-start.11
  192.7 12.1 %all-to-all-start.2 = ((bf16[8,2,512]{2,1,0:T(2,128)(2,1)}), bf16[8,2,512]{2,1,0:T(2,128)(2,1)S(1)}, u32[]{:S(2)}, u32[]{:S(2)}) async-start(bf16[8,2,512]{2,1,0:T(2,128)(2,1)} %convert_element_type.128), calls=%async_computation.3 | async-start | bytes 32768 | tf_op jit(solution)/shard_map/all_to_all | solution.py:129
Sparse Core Ops, SparseCore 0:
  27.6 68.1 all-reduce.2
  174.0 17.0 reduce-scatter.1
where the time goes:
time: 218 us; the launch traced here: 217 us
  waiting for transfers between devices  97.8 us (45%)
  blocking collectives  67.7 us (31%)
  starting transfers between devices  16.2 us (7%)
  between operations  15 us (7%)
  other arithmetic  7.82 us (4%)
  matrix products  6.92 us (3%)
  local copies, waits for them, and re-layouts  6.05 us (3%)
    unnamed x3, waiting for transfers between devices  68.3 us
    all_gather x1, blocking collectives, on_device(): lax.all_gather(moe_in, 'ep', axis=0, tiled=True)  30.5 us
    all_gather x1, blocking collectives, on_device(): lax.all_gather(gated_heads, 'ep', axis=0, tiled=True)  26.1 us
    reduce_scatter x1, waiting for transfers between devices, on_device(): lax.psum_scatter(output.astype(jnp.bfloat16), 'tp', scatter_dimension=1,...  16.2 us
    all_to_all x1, starting transfers between devices, on_device(): lax.all_to_all(normed, 'ep', split_axis=1, concat_axis=0, tiled=True)  7.31 us
    psum x1, blocking collectives, on_device(): lax.psum(returned.astype(jnp.float32).astype(jnp.bfloat16), 'tp')  5.87 us
    all_to_all x1, starting transfers between devices, on_device(): lax.all_to_all(outgoing.astype(jnp.bfloat16), 'ep', split_axis=0, concat_...  5.52 us
    all_to_all x1, waiting for transfers between devices, on_device(): lax.all_to_all(outgoing.astype(jnp.bfloat16), 'ep', split_axis=0, concat_...  5.4 us
  transfers between devices with their start and end apart: 5, of which 5 were waited for; matrix products, arithmetic and copies ran while one was open for 2% of the time, Pallas kernels for 0%

commit v1 on v0

v1 whole, which is shorter than its diff:
```python
import functools

import jax
import jax.numpy as jnp
from jax import lax
from jax.experimental import pallas as pl
from jax.experimental.pallas import tpu as pltpu
from jax.sharding import PartitionSpec as P

EPSILON = 1e-06
GATE_SCALE = 16.0
F32 = jnp.float32
BF16 = jnp.bfloat16
LANES = 128
MESH = pl.DeviceIdType.MESH


def mm(left, right):
    return jnp.dot(left, right, preferred_element_type=F32)


def over_peers(count, body):
    if count <= 8:
        for d in range(1, count):
            body(d)
    else:

        def step(d, carry):
            body(d)
            return carry

        lax.fori_loop(1, count, step, 0)


def over_range(count, body):
    for i in range(count):
        body(i)


def take_cols(ref, index, cols):
    if cols % LANES == 0:
        return ref[:, pl.ds(pl.multiple_of(index * cols, LANES), cols)]
    rows = ref.shape[1]
    select = (
        lax.broadcasted_iota(jnp.int32, (rows, cols), 0)
        == lax.broadcasted_iota(jnp.int32, (rows, cols), 1) + index * cols
    )
    return mm(ref[...], jnp.where(select, 1.0, 0.0).astype(BF16)).astype(BF16)


def kernel(
    n,
    t,
    residual_in,
    gla_state,
    norm_gain,
    w_query,
    w_key,
    w_value,
    w_decay,
    decay_bias,
    head_gain,
    w_output,
    ffn_gain,
    router_group,
    router_expert,
    expert_ids,
    w_gate,
    w_up,
    w_down,
    layer_out,
    new_state,
    res,
    state,
    ng,
    wcat,
    bias,
    hg,
    wo,
    fg,
    rg,
    re,
    ids,
    wgu,
    wd,
    load_sem,
    out_sem,
    a_rx,
    b_tx,
    b_rx,
    c_tx,
    c_rx,
    d1_rx,
    d1_tx,
    d2_rx,
    f1_tx,
    f1_rx,
    f2_rx,
    f2_tx,
    lout,
    rows_a,
    rows_c,
    heads8,
    proj,
    moe_out,
    ep_send,
    ep_recv,
    tp_send,
    tp_recv,
):
    e = lax.axis_index("ep")
    h = lax.axis_index("tp")
    seqs, width = res.shape
    cols = wcat.shape[0]
    kw = w_query.shape[1]
    vw = w_value.shape[1]
    tokens = n * seqs
    ff = wd.shape[0]
    aligned = cols % LANES == 0

    loads = []

    def load(src, dst):
        copy = pltpu.make_async_copy(src, dst, load_sem.at[len(loads)])
        copy.start()
        loads.append(copy)
        return copy

    ld_res = load(residual_in, res)
    ld_ng = load(norm_gain, ng)
    ld_w = [
        load(w_query, wcat.at[:, 0:kw]),
        load(w_key, wcat.at[:, kw : 2 * kw]),
        load(w_value, wcat.at[:, 2 * kw : 2 * kw + vw]),
        load(w_decay, wcat.at[:, 2 * kw + vw :]),
    ]
    ld_small = [load(decay_bias, bias), load(head_gain, hg), load(ffn_gain, fg)]
    ld_state = load(gla_state.at[:, 0], state)
    ld_wo = load(w_output, wo)
    ld_route = [load(router_group, rg), load(router_expert, re), load(expert_ids, ids)]
    ld_gu = [load(w_gate.at[0], wgu.at[:, 0:ff]), load(w_up.at[0], wgu.at[:, ff : 2 * ff])]
    ld_wd = load(w_down.at[0], wd)

    barrier = pltpu.get_barrier_semaphore()
    over_peers(
        n,
        lambda d: pl.semaphore_signal(
            barrier, inc=1, device_id={"ep": lax.rem(e + d, n)}, device_id_type=MESH
        ),
    )
    over_peers(
        t,
        lambda d: pl.semaphore_signal(
            barrier, inc=1, device_id={"tp": lax.rem(h + d, t)}, device_id_type=MESH
        ),
    )

    def ep_copy(phase, src, dst, peer, slot):
        return pltpu.make_async_remote_copy(
            src_ref=src,
            dst_ref=dst,
            send_sem=ep_send.at[phase, peer],
            recv_sem=ep_recv.at[phase, slot],
            device_id={"ep": peer},
            device_id_type=MESH,
        )

    def tp_copy(phase, src, dst, peer, slot):
        return pltpu.make_async_remote_copy(
            src_ref=src,
            dst_ref=dst,
            send_sem=tp_send.at[phase, peer],
            recv_sem=tp_recv.at[phase, slot],
            device_id={"tp": peer},
            device_id_type=MESH,
        )

    def ep_src(tx):
        return lambda peer: tx.at[peer]

    def ep_phase_send(phase, src_of, rx):
        def one(d):
            peer = lax.rem(e + d, n)
            ep_copy(phase, src_of(peer), rx.at[e], peer, e).start()

        over_peers(n, one)

    def ep_wait(phase, rx, peer):
        ep_copy(phase, rx.at[peer], rx.at[peer], peer, peer).wait_recv()

    def ep_drain(phase, src_of, rx):
        def one(d):
            peer = lax.rem(e + d, n)
            ep_copy(phase, src_of(peer), rx.at[e], peer, e).wait_send()

        over_peers(n, one)

    def tp_phase_send(phase, src, rx):
        def one(d):
            peer = lax.rem(h + d, t)
            tp_copy(phase, src, rx.at[h], peer, h).start()

        over_peers(t, one)

    def tp_wait_all(phase, rx):
        def one(d):
            peer = lax.rem(h + d, t)
            tp_copy(phase, rx.at[peer], rx.at[peer], peer, peer).wait_recv()

        over_peers(t, one)

    def tp_drain(phase, src, rx):
        def one(d):
            peer = lax.rem(h + d, t)
            tp_copy(phase, src, rx.at[h], peer, h).wait_send()

        over_peers(t, one)

    if aligned:
        a_src = lambda peer: res.at[:, pl.ds(pl.multiple_of(peer * cols, LANES), cols)]
    else:
        a_src = lambda peer: res
    ld_res.wait()
    pl.semaphore_wait(barrier, n - 1 + t - 1)
    ep_phase_send(0, a_src, a_rx)
    own = res[...]
    a_rx[e] = take_cols(res, e, cols) if aligned else own
    own_float = own.astype(F32)
    token_scale = lax.rsqrt(jnp.mean(own_float * own_float, axis=-1, keepdims=True) + EPSILON)
    ld_ng.wait()
    ng_cols = take_cols(ng, e, cols).astype(F32)
    for copy in ld_w:
        copy.wait()
    over_peers(n, lambda d: ep_wait(0, a_rx, lax.rem(e + d, n)))

    def fill_a(i):
        if aligned:
            piece = a_rx[i]
        else:
            piece = take_cols(a_rx.at[i], e, cols)
        rows_a[pl.ds(i * seqs, seqs), :] = piece.astype(F32)

    over_range(n, fill_a)

    lhs = (rows_a[...] * ng_cols).astype(BF16)
    proj[...] = mm(lhs, wcat[...])

    def fill_b(i):
        b_tx[i] = proj[pl.ds(i * seqs, seqs), :].astype(BF16)

    over_range(n, fill_b)
    ep_phase_send(1, ep_src(b_tx), b_rx)
    for copy in ld_small:
        copy.wait()
    ld_state.wait()
    b_rx[e] = b_tx[e]
    over_peers(n, lambda d: ep_wait(1, b_rx, lax.rem(e + d, n)))
    total = jnp.sum(b_rx[...].astype(F32), axis=0) * token_scale

    heads8[...] = jnp.zeros_like(heads8)
    decay_pre = total[:, 2 * kw + vw :] + bias[...]
    log_decay = (
        jnp.minimum(decay_pre, 0.0) - jnp.log1p(jnp.exp(-jnp.abs(decay_pre)))
    ) / GATE_SCALE
    heads8[0:seqs, :] = total[:, 0:kw] * kw ** (-0.5)
    heads8[seqs : 2 * seqs, :] = total[:, kw : 2 * kw]
    heads8[2 * seqs : 3 * seqs, :] = jnp.exp(log_decay)
    turned = heads8[...].T
    value_rows = total[:, 2 * kw : 2 * kw + vw]
    for b in range(seqs):
        value = value_rows[b : b + 1]
        acc = jnp.zeros((8, vw), F32)
        chunk = 64
        for c in range(0, kw, chunk):
            q_col = turned[c : c + chunk, b : b + 1]
            k_col = turned[c : c + chunk, seqs + b : seqs + b + 1]
            a_col = turned[c : c + chunk, 2 * seqs + b : 2 * seqs + b + 1]
            fresh = a_col * state[b, c : c + chunk, :] + k_col * value
            state[b, c : c + chunk, :] = fresh
            acc = acc + jnp.sum((q_col * fresh).reshape(chunk // 8, 8, vw), axis=0)
        read = jnp.sum(acc, axis=0, keepdims=True)
        gated = read * lax.rsqrt(jnp.mean(read * read, axis=-1, keepdims=True) + EPSILON)
        gated = gated * hg[...].astype(F32)
        rows_c[b : b + 1, :] = gated
    c_tx[...] = rows_c[0:seqs, :].astype(BF16)

    c_src = lambda peer: c_tx
    ep_phase_send(2, c_src, c_rx)
    st_out = pltpu.make_async_copy(state, new_state.at[:, 0], out_sem.at[0])
    st_out.start()
    c_rx[e] = c_tx[...]
    ld_wo.wait()
    over_peers(n, lambda d: ep_wait(2, c_rx, lax.rem(e + d, n)))

    def fill_c(i):
        rows_c[pl.ds(i * seqs, seqs), :] = c_rx[i].astype(F32)

    over_range(n, fill_c)

    part = mm(rows_c[...].astype(BF16), wo[...]).astype(BF16)
    d1_tx[...] = part
    tp_phase_send(0, d1_tx, d1_rx)
    d1_rx[h] = part
    tp_wait_all(0, d1_rx)
    attention = jnp.sum(d1_rx[...].astype(F32), axis=0)
    hid = (rows_a[...] + attention).astype(BF16)
    d2_rx[e] = hid
    d2_src = lambda peer: d2_rx.at[e]
    ep_phase_send(3, d2_src, d2_rx)
    for copy in ld_route + ld_gu:
        copy.wait()

    square = jnp.zeros((tokens, 1), F32)
    gate_up = jnp.zeros((tokens, 2 * ff), F32)
    group_logits = jnp.zeros((tokens, rg.shape[1]), F32)
    expert_logits = jnp.zeros((tokens, re.shape[0]), F32)

    def moe_chunk(d, carry):
        square, gate_up, group_logits, expert_logits = carry
        src = lax.rem(e + d, n)
        piece = d2_rx[src].astype(F32)
        square = square + jnp.sum(piece * piece, axis=-1, keepdims=True)
        piece = (piece * take_cols(fg, src, cols).astype(F32)).astype(BF16)
        span = pl.ds(pl.multiple_of(src * cols, cols), cols)
        gate_up = gate_up + mm(piece, wgu[span, :])
        group_logits = group_logits + mm(piece, rg[span, :])
        expert_logits = expert_logits + lax.dot_general(
            piece,
            take_cols(re, src, cols),
            (((1,), (1,)), ((), ())),
            preferred_element_type=F32,
        )
        return square, gate_up, group_logits, expert_logits

    def moe_step(d, carry):
        ep_wait(3, d2_rx, lax.rem(e + d, n))
        return moe_chunk(d, carry)

    carry = moe_chunk(0, (square, gate_up, group_logits, expert_logits))
    if n <= 8:
        for d in range(1, n):
            carry = moe_step(d, carry)
    else:
        carry = lax.fori_loop(1, n, moe_step, carry)
    square, gate_up, group_logits, expert_logits = carry
    scale = lax.rsqrt(square / (n * cols) + EPSILON)
    gate_up = gate_up * scale
    group_logits = group_logits * scale
    expert_logits = expert_logits * scale

    groups = group_logits.shape[1]
    experts = expert_logits.shape[1]
    first, second = ids[:, 0:1], ids[:, 1:2]
    named = (first == e) | (second == e)
    rival = jnp.where(first == e, second, first)
    expert_at = lax.broadcasted_iota(jnp.int32, expert_logits.shape, 1)
    group_at = lax.broadcasted_iota(jnp.int32, group_logits.shape, 1)
    pick = lambda mask, values: jnp.sum(jnp.where(mask, values, 0.0), axis=1, keepdims=True)
    chosen = pick(expert_at == e, expert_logits)
    rival_logit = pick(expert_at == rival, expert_logits)
    group_logit = pick(group_at == e // (experts // groups), group_logits)
    share = 1.0 / jnp.sum(jnp.exp(group_logits - group_logit), axis=1, keepdims=True)
    weight = jnp.where(named, share / (1.0 + jnp.exp(rival_logit - chosen)), 0.0)

    gate, up = gate_up[:, 0:ff], gate_up[:, ff : 2 * ff]
    hidden = (gate / (1.0 + jnp.exp(-gate)) * up).astype(BF16)
    ld_wd.wait()
    moe_out[...] = mm(hidden, wd[...]) * weight

    def fill_f(i):
        f1_tx[i] = moe_out[pl.ds(i * seqs, seqs), :].astype(BF16)

    over_range(n, fill_f)
    f1_src = ep_src(f1_tx)
    ep_phase_send(4, f1_src, f1_rx)
    f1_rx[e] = f1_tx[e]
    own_rows = (
        lax.broadcasted_iota(jnp.int32, (8, tokens), 1)
        == lax.broadcasted_iota(jnp.int32, (8, tokens), 0) + e * seqs
    )
    own_rows = jnp.where(own_rows, 1.0, 0.0).astype(BF16)
    if aligned:
        for i in range(n):
            lout[:, i * cols : (i + 1) * cols] = mm(own_rows, d2_rx[i])[0:seqs]
    over_peers(n, lambda d: ep_wait(4, f1_rx, lax.rem(e + d, n)))
    f2_tx[...] = jnp.sum(f1_rx[...].astype(F32), axis=0).astype(BF16)
    tp_phase_send(1, f2_tx, f2_rx)
    f2_rx[h] = f2_tx[...]
    tp_wait_all(1, f2_rx)
    if not aligned:

        def place(i, total_rows):
            rows = mm(own_rows, d2_rx[i]).astype(BF16)
            select = (
                lax.broadcasted_iota(jnp.int32, (cols, width), 1)
                == lax.broadcasted_iota(jnp.int32, (cols, width), 0) + i * cols
            )
            return total_rows + mm(rows, jnp.where(select, 1.0, 0.0).astype(BF16))

        lout[...] = lax.fori_loop(0, n, place, jnp.zeros((8, width), F32))[0:seqs]
    moe_sum = jnp.sum(f2_rx[...].astype(F32), axis=0)
    layer_out[...] = (lout[...] + moe_sum).astype(BF16)

    ep_drain(0, a_src, a_rx)
    ep_drain(1, ep_src(b_tx), b_rx)
    ep_drain(2, c_src, c_rx)
    ep_drain(3, d2_src, d2_rx)
    ep_drain(4, f1_src, f1_rx)
    tp_drain(0, d1_tx, d1_rx)
    tp_drain(1, f2_tx, f2_rx)
    st_out.wait()


def on_device(n, t, *arrays):
    (
        residual_in,
        gla_state,
        norm_gain,
        w_query,
        w_key,
        w_value,
        w_decay,
        decay_bias,
        head_gain,
        w_output,
        ffn_gain,
        router_group,
        router_expert,
        expert_ids,
        w_gate,
        w_up,
        w_down,
    ) = arrays
    seqs, width = residual_in.shape
    tokens = n * seqs
    cols, kw = w_query.shape
    vw = w_value.shape[1]
    ff = w_gate.shape[2]
    span = 3 * kw + vw
    out_cols = w_output.shape[1]
    a_cols = cols if cols % LANES == 0 else width
    row = lambda a: a.reshape(1, -1)
    operands = (
        residual_in,
        gla_state,
        row(norm_gain),
        w_query,
        w_key,
        w_value,
        w_decay,
        row(decay_bias),
        row(head_gain),
        w_output,
        row(ffn_gain),
        router_group,
        router_expert,
        expert_ids,
        w_gate,
        w_up,
        w_down,
    )
    dma = pltpu.SemaphoreType.DMA
    scratch = [
        pltpu.VMEM((seqs, width), BF16),
        pltpu.VMEM((seqs, kw, vw), F32),
        pltpu.VMEM((1, width), BF16),
        pltpu.VMEM((cols, span), BF16),
        pltpu.VMEM((1, kw), F32),
        pltpu.VMEM((1, vw), BF16),
        pltpu.VMEM(w_output.shape, BF16),
        pltpu.VMEM((1, width), BF16),
        pltpu.VMEM(router_group.shape, BF16),
        pltpu.VMEM(router_expert.shape, BF16),
        pltpu.VMEM(expert_ids.shape, jnp.int32),
        pltpu.VMEM((width, 2 * ff), BF16),
        pltpu.VMEM((ff, width), BF16),
        dma((17,)),
        dma((1,)),
        pltpu.VMEM((n, seqs, a_cols), BF16),
        pltpu.VMEM((n, seqs, span), BF16),
        pltpu.VMEM((n, seqs, span), BF16),
        pltpu.VMEM((seqs, vw), BF16),
        pltpu.VMEM((n, seqs, vw), BF16),
        pltpu.VMEM((t, tokens, out_cols), BF16),
        pltpu.VMEM((tokens, out_cols), BF16),
        pltpu.VMEM((n, tokens, out_cols), BF16),
        pltpu.VMEM((n, seqs, width), BF16),
        pltpu.VMEM((n, seqs, width), BF16),
        pltpu.VMEM((t, seqs, width), BF16),
        pltpu.VMEM((seqs, width), BF16),
        pltpu.VMEM((seqs, width), F32),
        pltpu.VMEM((tokens, cols), F32),
        pltpu.VMEM((tokens, vw), F32),
        pltpu.VMEM((8, kw), F32),
        pltpu.VMEM((tokens, span), F32),
        pltpu.VMEM((tokens, width), F32),
        dma((5, n)),
        dma((5, n)),
        dma((2, t)),
        dma((2, t)),
    ]
    layer_out, new_state = pl.pallas_call(
        functools.partial(kernel, n, t),
        out_shape=(
            jax.ShapeDtypeStruct((seqs, width), BF16),
            jax.ShapeDtypeStruct(gla_state.shape, F32),
        ),
        in_specs=[pl.BlockSpec(memory_space=pl.ANY)] * len(operands),
        out_specs=(
            pl.BlockSpec(memory_space=pltpu.VMEM),
            pl.BlockSpec(memory_space=pl.ANY),
        ),
        scratch_shapes=scratch,
        compiler_params=pltpu.CompilerParams(
            collective_id=0, has_side_effects=True, vmem_limit_bytes=56 * 1024 * 1024
        ),
    )(*operands)
    return layer_out, new_state


def solution(mesh):
    n, t = mesh.shape["ep"], mesh.shape["tp"]
    placed = (
        P("ep", None),
        P("ep", "tp", None, None),
        P(),
        P("ep", "tp"),
        P("ep", "tp"),
        P("ep", "tp"),
        P("ep", "tp"),
        P("tp"),
        P(),
        P("tp", "ep"),
        P(),
        P(),
        P(),
        P(),
        P("ep", None, "tp"),
        P("ep", None, "tp"),
        P("ep", "tp", None),
    )
    return jax.shard_map(
        functools.partial(on_device, n, t),
        mesh=mesh,
        in_specs=placed,
        out_specs=(P("ep", None), P("ep", "tp", None, None)),
        check_vma=False,
    )
```

time: 218 us -> 44.2 us (0.20)
  waiting for transfers between devices: 97.8 us -> 0 us
  blocking collectives: 67.7 us -> 0 us
  Pallas kernels: 0 us -> 35.4 us
  starting transfers between devices: 16.2 us -> 0 us
  between operations: 15 us -> 0.66 us
  other arithmetic: 7.82 us -> 0 us
  matrix products: 6.92 us -> 0 us
    unnamed x3 -> x0, waiting for transfers between devices: 68.3 us -> none
    all_gather x3 -> x0, blocking collectives: 61.8 us -> none  [the longest x1 30.5 us: on_device(): lax.all_gather(moe_in, 'ep', axis=0, tiled=True)]
    pallas_call x0 -> x1, Pallas kernels: none -> 35.4 us  [on_device(): pl.pallas_call(functools.partial(kernel, n, t), out_shape=(jax.ShapeDtype...]
    reduce_scatter x1 -> x0, waiting for transfers between devices: 16.2 us -> none  [on_device(): lax.psum_scatter(output.astype(jnp.bfloat16), 'tp', scatter_dimension=1,...]
    all_to_all x3 -> x0, starting transfers between devices: 16.2 us -> none  [the longest x1 7.31 us: on_device(): lax.all_to_all(normed, 'ep', split_axis=1, concat_axis=0, tiled=True)]
    all_to_all x3 -> x0, waiting for transfers between devices: 13.3 us -> none  [the longest x1 5.4 us: on_device(): lax.all_to_all(outgoing.astype(jnp.bfloat16), 'ep', split_axis=0, concat_...]
    dot_general x12 -> x0, matrix products: 6.92 us -> none  [the longest x1 1.1 us: on_device(): jnp.dot(columns, w_value, preferred_element_type=jnp.float32)]
    psum x1 -> x0, blocking collectives: 5.87 us -> none  [on_device(): lax.psum(returned.astype(jnp.float32).astype(jnp.bfloat16), 'tp')]
  transfers between devices with their start and end apart: 5 -> 0, of which waited for: 5 -> 0; matrix products, arithmetic and copies ran while one was open for 2% -> 0% of each run, Pallas kernels for 0% -> 0%
where the time goes in v1:
time: 44.2 us; the launch traced here: 43.9 us
  Pallas kernels  35.4 us (80%)
  local copies, waits for them, and re-layouts  7.85 us (18%)
  between operations  0.66 us (1%)
    pallas_call x1, Pallas kernels, on_device(): pl.pallas_call(functools.partial(kernel, n, t), out_shape=(jax.ShapeDtype...  35.4 us
    unnamed x12, local copies, waits for them, and re-layouts  5.38 us
    reshape x3, local copies, waits for them, and re-layouts, on_device(): row = lambda a: a.reshape(1, -1)  2.47 us

profile of v1, /device:TPU:0, one launch (start us, length us, event | category | flops | bytes accessed | tf_op | source)
XLA Modules:
  0.0 43.9 jit_solution(6320761784358268350)
XLA Ops:
  0.6 0.0 copy-start.1
  0.6 0.0 copy-start.2
  0.7 1.3 %reshape.18.head_gain = bf16[1,512]{1,0:T(2,128)(2,1)} reshape(bf16[512]{0:T(512)(128)(2,1)} %param.25) | data formatting | bytes 2048 | tf_op jit(solution)/shard_map/reshape | solution.py:442
  1.9 0.0 copy-done.1
  1.9 0.0 copy-start
  1.9 0.6 %reshape.16.norm_gain = bf16[1,2048]{1,0:T(2,128)(2,1)} reshape(bf16[2048]{0:T(1024)(128)(2,1)S(1)} %copy-done.1) | data formatting | bytes 8192 | tf_op jit(solution)/shard_map/reshape | solution.py:442
  2.5 0.0 copy-done.2
  2.5 0.0 copy-start.3
  2.5 0.6 %reshape.19.ffn_gain = bf16[1,2048]{1,0:T(2,128)(2,1)} reshape(bf16[2048]{0:T(1024)(128)(2,1)S(1)} %copy-done.2) | data formatting | bytes 8192 | tf_op jit(solution)/shard_map/reshape | solution.py:442
  3.1 0.1 copy-done.3
  3.2 0.7 %copy.20.expert_ids = s32[16,2]{1,0:T(8,128)} copy(s32[16,2]{0,1:T(2,128)S(1)} %copy-done.3) | data formatting | bytes 256 | tf_op args[13]
  3.9 0.0 copy-done
  3.9 1.1 %copy.19.router_group = bf16[2048,4]{1,0:T(8,128)(2,1)} copy(bf16[2048,4]{0,1:T(4,128)(2,1)S(1)} %copy-done) | data formatting | bytes 32768 | tf_op args[11]
  4.9 35.4 %shard_map.176 = (bf16[2,2048]{1,0:T(2,128)(2,1)}, f32[2,1,256,512]{3,2,1,0:T(8,128)}) custom-call(bf16[2,2048]{1,0:T(2,128)(2,1)} %residual_in.1, f32[2,1,256,512]{3,2,1,0:T(8,128)} %gla_state.1, bf16[1,2048]{1,0:T(2,128)(2,1)} %reshape.16.norm_gain, bf16[256,256]{1,0:T(8,128)(2,1)} %w_query.1, bf16[256,256]{1,0:T(8,128)(2,1)} %w_key.1, ...), custom_call_target="tpu_custom_call" | custom-call | tf_op jit(solution)/shard_map/pallas_call | solution.py:502
  40.3 1.3 %copy.23 = bf16[2,2048]{1,0:T(2,128)(2,1)} copy(bf16[2,2048]{1,0:T(2,128)(2,1)} %get-tuple-element.4) | data formatting | bytes 16384
  41.6 2.3 %copy.24 = f32[2,1,256,512]{3,2,1,0:T(8,128)} copy(f32[2,1,256,512]{3,2,1,0:T(8,128)} %get-tuple-element.5) | data formatting | bytes 2097152
Async XLA Ops:
  0.6 1.3 %copy-start.1 = (bf16[2048]{0:T(1024)(128)(2,1)S(1)}, bf16[2048]{0:T(1024)(128)(2,1)}, u32[]{:S(2)}) copy-start(bf16[2048]{0:T(1024)(128)(2,1)} %param.19) | copy-start | bytes 12292
  0.6 1.9 %copy-start.2 = (bf16[2048]{0:T(1024)(128)(2,1)S(1)}, bf16[2048]{0:T(1024)(128)(2,1)}, u32[]{:S(2)}) copy-start(bf16[2048]{0:T(1024)(128)(2,1)} %param.27) | copy-start | bytes 12292
  1.9 2.0 %copy-start = (bf16[2048,4]{0,1:T(4,128)(2,1)S(1)}, bf16[2048,4]{0,1:T(4,128)(2,1)}, u32[]{:S(2)}) copy-start(bf16[2048,4]{0,1:T(4,128)(2,1)} %param.28) | copy-start | bytes 49156
  2.5 0.7 %copy-start.3 = (s32[16,2]{0,1:T(2,128)S(1)}, s32[16,2]{0,1:T(2,128)}, u32[]{:S(2)}) copy-start(s32[16,2]{0,1:T(2,128)} %param.30) | copy-start | bytes 388

commit v2 on v1

--- a/solution.py
+++ b/solution.py
@@ -19,17 +19,36 @@
     return jnp.dot(left, right, preferred_element_type=F32)
 
 
-def over_peers(count, body):
+def mm_nt(left, right):
+    return lax.dot_general(
+        left, right, (((1,), (1,)), ((), ())), preferred_element_type=F32
+    )
+
+
+def over_peers(me, count, body, far_first=False):
     if count <= 8:
-        for d in range(1, count):
-            body(d)
+        order = range(1, count)
+        for d in reversed(order) if far_first else order:
+            body(flip(me, count, d))
     else:
 
         def step(d, carry):
-            body(d)
+            body(lax.rem(me + d, count))
             return carry
 
         lax.fori_loop(1, count, step, 0)
+
+
+def flip(me, count, d):
+    if count & (count - 1):
+        return lax.rem(me + d, count)
+    peer = me
+    bit = 1
+    while bit < count:
+        if d & bit:
+            peer = peer + bit - 2 * bit * ((me // bit) % 2)
+        bit *= 2
+    return peer
 
 
 def over_range(count, body):
@@ -45,7 +64,12 @@
         lax.broadcasted_iota(jnp.int32, (rows, cols), 0)
         == lax.broadcasted_iota(jnp.int32, (rows, cols), 1) + index * cols
     )
-    return mm(ref[...], jnp.where(select, 1.0, 0.0).astype(BF16)).astype(BF16)
+    return mm(ref[...].astype(BF16), jnp.where(select, 1.0, 0.0).astype(BF16)).astype(BF16)
+
+
+def as_row(ref):
+    values = ref[...].astype(F32)
+    return jnp.concatenate([values[r : r + 1] for r in range(values.shape[0])], axis=1)
 
 
 def kernel(
@@ -73,11 +97,13 @@
     res,
     state,
     ng,
+    ng_row,
     wcat,
     bias,
     hg,
     wo,
     fg,
+    fg_row,
     rg,
     re,
     ids,
@@ -118,6 +144,16 @@
     ff = wd.shape[0]
     aligned = cols % LANES == 0
 
+    barrier = pltpu.get_barrier_semaphore()
+
+    def greet(axis):
+        return lambda peer: pl.semaphore_signal(
+            barrier, inc=1, device_id={axis: peer}, device_id_type=MESH
+        )
+
+    over_peers(e, n, greet("ep"), far_first=True)
+    over_peers(h, t, greet("tp"))
+
     loads = []
 
     def load(src, dst):
@@ -141,20 +177,6 @@
     ld_gu = [load(w_gate.at[0], wgu.at[:, 0:ff]), load(w_up.at[0], wgu.at[:, ff : 2 * ff])]
     ld_wd = load(w_down.at[0], wd)
 
-    barrier = pltpu.get_barrier_semaphore()
-    over_peers(
-        n,
-        lambda d: pl.semaphore_signal(
-            barrier, inc=1, device_id={"ep": lax.rem(e + d, n)}, device_id_type=MESH
-        ),
-    )
-    over_peers(
-        t,
-        lambda d: pl.semaphore_signal(
-            barrier, inc=1, device_id={"tp": lax.rem(h + d, t)}, device_id_type=MESH
-        ),
-    )
-
     def ep_copy(phase, src, dst, peer, slot):
         return pltpu.make_async_remote_copy(
             src_ref=src,
@@ -179,42 +201,38 @@
         return lambda peer: tx.at[peer]
 
     def ep_phase_send(phase, src_of, rx):
-        def one(d):
-            peer = lax.rem(e + d, n)
-            ep_copy(phase, src_of(peer), rx.at[e], peer, e).start()
-
-        over_peers(n, one)
+        over_peers(
+            e,
+            n,
+            lambda peer: ep_copy(phase, src_of(peer), rx.at[e], peer, e).start(),
+            far_first=True,
+        )
 
     def ep_wait(phase, rx, peer):
         ep_copy(phase, rx.at[peer], rx.at[peer], peer, peer).wait_recv()
 
+    def ep_wait_all(phase, rx):
+        over_peers(e, n, lambda peer: ep_wait(phase, rx, peer))
+
     def ep_drain(phase, src_of, rx):
-        def one(d):
-            peer = lax.rem(e + d, n)
-            ep_copy(phase, src_of(peer), rx.at[e], peer, e).wait_send()
-
-        over_peers(n, one)
+        over_peers(
+            e, n, lambda peer: ep_copy(phase, src_of(peer), rx.at[e], peer, e).wait_send()
+        )
 
     def tp_phase_send(phase, src, rx):
-        def one(d):
-            peer = lax.rem(h + d, t)
-            tp_copy(phase, src, rx.at[h], peer, h).start()
-
-        over_peers(t, one)
+        over_peers(
+            h, t, lambda peer: tp_copy(phase, src, rx.at[h], peer, h).start(), far_first=True
+        )
 
     def tp_wait_all(phase, rx):
-        def one(d):
-            peer = lax.rem(h + d, t)
-            tp_copy(phase, rx.at[peer], rx.at[peer], peer, peer).wait_recv()
-
-        over_peers(t, one)
+        over_peers(
+            h, t, lambda peer: tp_copy(phase, rx.at[peer], rx.at[peer], peer, peer).wait_recv()
+        )
 
     def tp_drain(phase, src, rx):
-        def one(d):
-            peer = lax.rem(h + d, t)
-            tp_copy(phase, src, rx.at[h], peer, h).wait_send()
-
-        over_peers(t, one)
+        over_peers(
+            h, t, lambda peer: tp_copy(phase, src, rx.at[h], peer, h).wait_send()
+        )
 
     if aligned:
         a_src = lambda peer: res.at[:, pl.ds(pl.multiple_of(peer * cols, LANES), cols)]
@@ -228,10 +246,11 @@
     own_float = own.astype(F32)
     token_scale = lax.rsqrt(jnp.mean(own_float * own_float, axis=-1, keepdims=True) + EPSILON)
     ld_ng.wait()
-    ng_cols = take_cols(ng, e, cols).astype(F32)
+    ng_row[...] = as_row(ng)
+    ng_cols = take_cols(ng_row, e, cols).astype(F32)
     for copy in ld_w:
         copy.wait()
-    over_peers(n, lambda d: ep_wait(0, a_rx, lax.rem(e + d, n)))
+    ep_wait_all(0, a_rx)
 
     def fill_a(i):
         if aligned:
@@ -253,8 +272,11 @@
     for copy in ld_small:
         copy.wait()
     ld_state.wait()
+    for copy in ld_route + ld_gu:
+        copy.wait()
+    fg_row[...] = as_row(fg)
     b_rx[e] = b_tx[e]
-    over_peers(n, lambda d: ep_wait(1, b_rx, lax.rem(e + d, n)))
+    ep_wait_all(1, b_rx)
     total = jnp.sum(b_rx[...].astype(F32), axis=0) * token_scale
 
     heads8[...] = jnp.zeros_like(heads8)
@@ -266,6 +288,7 @@
     heads8[seqs : 2 * seqs, :] = total[:, kw : 2 * kw]
     heads8[2 * seqs : 3 * seqs, :] = jnp.exp(log_decay)
     turned = heads8[...].T
+    head_row = as_row(hg)
     value_rows = total[:, 2 * kw : 2 * kw + vw]
     for b in range(seqs):
         value = value_rows[b : b + 1]
@@ -280,7 +303,7 @@
             acc = acc + jnp.sum((q_col * fresh).reshape(chunk // 8, 8, vw), axis=0)
         read = jnp.sum(acc, axis=0, keepdims=True)
         gated = read * lax.rsqrt(jnp.mean(read * read, axis=-1, keepdims=True) + EPSILON)
-        gated = gated * hg[...].astype(F32)
+        gated = gated * head_row
         rows_c[b : b + 1, :] = gated
     c_tx[...] = rows_c[0:seqs, :].astype(BF16)
 
@@ -290,7 +313,7 @@
     st_out.start()
     c_rx[e] = c_tx[...]
     ld_wo.wait()
-    over_peers(n, lambda d: ep_wait(2, c_rx, lax.rem(e + d, n)))
+    ep_wait_all(2, c_rx)
 
     def fill_c(i):
         rows_c[pl.ds(i * seqs, seqs), :] = c_rx[i].astype(F32)
@@ -307,41 +330,33 @@
     d2_rx[e] = hid
     d2_src = lambda peer: d2_rx.at[e]
     ep_phase_send(3, d2_src, d2_rx)
-    for copy in ld_route + ld_gu:
-        copy.wait()
 
     square = jnp.zeros((tokens, 1), F32)
     gate_up = jnp.zeros((tokens, 2 * ff), F32)
-    group_logits = jnp.zeros((tokens, rg.shape[1]), F32)
+    group_logits = jnp.zeros((tokens, rg.shape[0]), F32)
     expert_logits = jnp.zeros((tokens, re.shape[0]), F32)
 
-    def moe_chunk(d, carry):
+    def moe_chunk(src, carry):
         square, gate_up, group_logits, expert_logits = carry
-        src = lax.rem(e + d, n)
         piece = d2_rx[src].astype(F32)
         square = square + jnp.sum(piece * piece, axis=-1, keepdims=True)
-        piece = (piece * take_cols(fg, src, cols).astype(F32)).astype(BF16)
+        piece = (piece * take_cols(fg_row, src, cols).astype(F32)).astype(BF16)
         span = pl.ds(pl.multiple_of(src * cols, cols), cols)
         gate_up = gate_up + mm(piece, wgu[span, :])
-        group_logits = group_logits + mm(piece, rg[span, :])
-        expert_logits = expert_logits + lax.dot_general(
-            piece,
-            take_cols(re, src, cols),
-            (((1,), (1,)), ((), ())),
-            preferred_element_type=F32,
-        )
+        group_logits = group_logits + mm_nt(piece, take_cols(rg, src, cols))
+        expert_logits = expert_logits + mm_nt(piece, take_cols(re, src, cols))
         return square, gate_up, group_logits, expert_logits
 
-    def moe_step(d, carry):
-        ep_wait(3, d2_rx, lax.rem(e + d, n))
-        return moe_chunk(d, carry)
-
-    carry = moe_chunk(0, (square, gate_up, group_logits, expert_logits))
+    def moe_step(src, carry):
+        ep_wait(3, d2_rx, src)
+        return moe_chunk(src, carry)
+
+    carry = moe_chunk(e, (square, gate_up, group_logits, expert_logits))
     if n <= 8:
         for d in range(1, n):
-            carry = moe_step(d, carry)
+            carry = moe_step(flip(e, n, d), carry)
     else:
-        carry = lax.fori_loop(1, n, moe_step, carry)
+        carry = lax.fori_loop(1, n, lambda d, c: moe_step(lax.rem(e + d, n), c), carry)
     square, gate_up, group_logits, expert_logits = carry
     scale = lax.rsqrt(square / (n * cols) + EPSILON)
     gate_up = gate_up * scale
@@ -350,7 +365,11 @@
 
     groups = group_logits.shape[1]
     experts = expert_logits.shape[1]
-    first, second = ids[:, 0:1], ids[:, 1:2]
+    diagonal = lax.broadcasted_iota(jnp.int32, (tokens, tokens), 0) == (
+        lax.broadcasted_iota(jnp.int32, (tokens, tokens), 1)
+    )
+    column = lambda row: jnp.sum(jnp.where(diagonal, row, 0), axis=1, keepdims=True)
+    first, second = column(ids[0:1, :]), column(ids[1:2, :])
     named = (first == e) | (second == e)
     rival = jnp.where(first == e, second, first)
     expert_at = lax.broadcasted_iota(jnp.int32, expert_logits.shape, 1)
@@ -374,6 +393,7 @@
     f1_src = ep_src(f1_tx)
     ep_phase_send(4, f1_src, f1_rx)
     f1_rx[e] = f1_tx[e]
+    ep_drain(0, a_src, a_rx)
     own_rows = (
         lax.broadcasted_iota(jnp.int32, (8, tokens), 1)
         == lax.broadcasted_iota(jnp.int32, (8, tokens), 0) + e * seqs
@@ -382,7 +402,7 @@
     if aligned:
         for i in range(n):
             lout[:, i * cols : (i + 1) * cols] = mm(own_rows, d2_rx[i])[0:seqs]
-    over_peers(n, lambda d: ep_wait(4, f1_rx, lax.rem(e + d, n)))
+    ep_wait_all(4, f1_rx)
     f2_tx[...] = jnp.sum(f1_rx[...].astype(F32), axis=0).astype(BF16)
     tp_phase_send(1, f2_tx, f2_rx)
     f2_rx[h] = f2_tx[...]
@@ -399,9 +419,10 @@
 
         lout[...] = lax.fori_loop(0, n, place, jnp.zeros((8, width), F32))[0:seqs]
     moe_sum = jnp.sum(f2_rx[...].astype(F32), axis=0)
-    layer_out[...] = (lout[...] + moe_sum).astype(BF16)
-
-    ep_drain(0, a_src, a_rx)
+    res[...] = (lout[...] + moe_sum).astype(BF16)
+    lo_out = pltpu.make_async_copy(res, layer_out, out_sem.at[1])
+    lo_out.start()
+
     ep_drain(1, ep_src(b_tx), b_rx)
     ep_drain(2, c_src, c_rx)
     ep_drain(3, d2_src, d2_rx)
@@ -409,6 +430,7 @@
     tp_drain(0, d1_tx, d1_rx)
     tp_drain(1, f2_tx, f2_rx)
     st_out.wait()
+    lo_out.wait()
 
 
 def on_device(n, t, *arrays):
@@ -439,22 +461,22 @@
     span = 3 * kw + vw
     out_cols = w_output.shape[1]
     a_cols = cols if cols % LANES == 0 else width
-    row = lambda a: a.reshape(1, -1)
+    lanes = lambda a: a.reshape(-1, LANES)
     operands = (
         residual_in,
         gla_state,
-        row(norm_gain),
+        lanes(norm_gain),
         w_query,
         w_key,
         w_value,
         w_decay,
-        row(decay_bias),
-        row(head_gain),
+        decay_bias.reshape(1, -1),
+        lanes(head_gain),
         w_output,
-        row(ffn_gain),
-        router_group,
+        lanes(ffn_gain),
+        router_group.T,
         router_expert,
-        expert_ids,
+        expert_ids.T,
         w_gate,
         w_up,
         w_down,
@@ -463,19 +485,21 @@
     scratch = [
         pltpu.VMEM((seqs, width), BF16),
         pltpu.VMEM((seqs, kw, vw), F32),
-        pltpu.VMEM((1, width), BF16),
+        pltpu.VMEM((width // LANES, LANES), BF16),
+        pltpu.VMEM((1, width), F32),
         pltpu.VMEM((cols, span), BF16),
         pltpu.VMEM((1, kw), F32),
-        pltpu.VMEM((1, vw), BF16),
+        pltpu.VMEM((vw // LANES, LANES), BF16),
         pltpu.VMEM(w_output.shape, BF16),
-        pltpu.VMEM((1, width), BF16),
-        pltpu.VMEM(router_group.shape, BF16),
+        pltpu.VMEM((width // LANES, LANES), BF16),
+        pltpu.VMEM((1, width), F32),
+        pltpu.VMEM(router_group.shape[::-1], BF16),
         pltpu.VMEM(router_expert.shape, BF16),
-        pltpu.VMEM(expert_ids.shape, jnp.int32),
+        pltpu.VMEM(expert_ids.shape[::-1], jnp.int32),
         pltpu.VMEM((width, 2 * ff), BF16),
         pltpu.VMEM((ff, width), BF16),
         dma((17,)),
-        dma((1,)),
+        dma((2,)),
         pltpu.VMEM((n, seqs, a_cols), BF16),
         pltpu.VMEM((n, seqs, span), BF16),
         pltpu.VMEM((n, seqs, span), BF16),
@@ -499,22 +523,23 @@
         dma((2, t)),
         dma((2, t)),
     ]
+    limit = (12 if n <= 8 else 48) * 1024 * 1024
     layer_out, new_state = pl.pallas_call(
         functools.partial(kernel, n, t),
         out_shape=(
             jax.ShapeDtypeStruct((seqs, width), BF16),
             jax.ShapeDtypeStruct(gla_state.shape, F32),
         ),
-        in_specs=[pl.BlockSpec(memory_space=pl.ANY)] * len(operands),
+        in_specs=[pl.BlockSpec(memory_space=pltpu.HBM)] * len(operands),
         out_specs=(
-            pl.BlockSpec(memory_space=pltpu.VMEM),
+            pl.BlockSpec(memory_space=pl.ANY),
             pl.BlockSpec(memory_space=pl.ANY),
         ),
         scratch_shapes=scratch,
         compiler_params=pltpu.CompilerParams(
-            collective_id=0, has_side_effects=True, vmem_limit_bytes=56 * 1024 * 1024
+            collective_id=0, has_side_effects=True, vmem_limit_bytes=limit
         ),
-    )(*operands)
+    )(*[pltpu.with_memory_space_constraint(a, pltpu.HBM) for a in operands])
     return layer_out, new_state
 
 

time: 44.2 us -> 36.2 us (0.82)
  local copies, waits for them, and re-layouts: 7.85 us -> 1.57 us
  Pallas kernels: 35.4 us -> 33.8 us
    unnamed x12 -> x2, local copies, waits for them, and re-layouts: 5.38 us -> 1.57 us
    reshape x3 -> x0, local copies, waits for them, and re-layouts: 2.47 us -> none  [on_device(): row = lambda a: a.reshape(1, -1)]
    pallas_call x1, Pallas kernels: 35.4 us -> 33.8 us  [on_device(): pl.pallas_call(functools.partial(kernel, n, t), out_shape=(jax.ShapeDtype...]
where the time goes in v2:
time: 36.2 us; the launch traced here: 36 us
  Pallas kernels  33.8 us (93%)
  local copies, waits for them, and re-layouts  1.57 us (4%)
  between operations  0.65 us (2%)
    pallas_call x1, Pallas kernels, on_device(): pl.pallas_call(functools.partial(kernel, n, t), out_shape=(jax.ShapeDtype...  33.8 us
    unnamed x2, local copies, waits for them, and re-layouts  1.57 us

profile of v2, /device:TPU:0, one launch (start us, length us, event | category | flops | bytes accessed | tf_op | source)
XLA Modules:
  0.0 36.0 jit_solution(13948848642727082803)
XLA Ops:
  0.6 33.8 %shard_map.176 = (bf16[2,2048]{1,0:T(2,128)(2,1)S(1)}, f32[2,1,256,512]{3,2,1,0:T(8,128)S(1)}) custom-call(bf16[2,2048]{1,0:T(2,128)(2,1)} %residual_in.1, f32[2,1,256,512]{3,2,1,0:T(8,128)} %gla_state.1, bf16[16,128]{1,0:T(8,128)(2,1)} %bitcast.7, bf16[256,256]{1,0:T(8,128)(2,1)} %w_query.1, bf16[256,256]{1,0:T(8,128)(2,1)} %w_key.1, ...), custom_call_target="tpu_custom_call" | custom-call | tf_op jit(solution)/shard_map/pallas_call | solution.py:527
  34.4 0.6 %copy.21 = bf16[2,2048]{1,0:T(2,128)(2,1)} copy(bf16[2,2048]{1,0:T(2,128)(2,1)S(1)} %get-tuple-element.4) | data formatting | bytes 16384
  35.0 1.0 %copy.22 = f32[2,1,256,512]{3,2,1,0:T(8,128)} copy(f32[2,1,256,512]{3,2,1,0:T(8,128)S(1)} %get-tuple-element.5) | data formatting | bytes 2097152

commit v3 on v2

--- a/solution.py
+++ b/solution.py
@@ -17,12 +17,6 @@
 
 def mm(left, right):
     return jnp.dot(left, right, preferred_element_type=F32)
-
-
-def mm_nt(left, right):
-    return lax.dot_general(
-        left, right, (((1,), (1,)), ((), ())), preferred_element_type=F32
-    )
 
 
 def over_peers(me, count, body, far_first=False):
@@ -106,6 +100,8 @@
     fg_row,
     rg,
     re,
+    both,
+    route,
     ids,
     wgu,
     wd,
@@ -118,6 +114,7 @@
     c_rx,
     d1_rx,
     d1_tx,
+    d2_tx,
     d2_rx,
     f1_tx,
     f1_rx,
@@ -144,16 +141,6 @@
     ff = wd.shape[0]
     aligned = cols % LANES == 0
 
-    barrier = pltpu.get_barrier_semaphore()
-
-    def greet(axis):
-        return lambda peer: pl.semaphore_signal(
-            barrier, inc=1, device_id={axis: peer}, device_id_type=MESH
-        )
-
-    over_peers(e, n, greet("ep"), far_first=True)
-    over_peers(h, t, greet("tp"))
-
     loads = []
 
     def load(src, dst):
@@ -163,6 +150,17 @@
         return copy
 
     ld_res = load(residual_in, res)
+
+    barrier = pltpu.get_barrier_semaphore()
+
+    def greet(axis):
+        return lambda peer: pl.semaphore_signal(
+            barrier, inc=1, device_id={axis: peer}, device_id_type=MESH
+        )
+
+    over_peers(e, n, greet("ep"), far_first=True)
+    over_peers(h, t, greet("tp"))
+
     ld_ng = load(norm_gain, ng)
     ld_w = [
         load(w_query, wcat.at[:, 0:kw]),
@@ -170,12 +168,6 @@
         load(w_value, wcat.at[:, 2 * kw : 2 * kw + vw]),
         load(w_decay, wcat.at[:, 2 * kw + vw :]),
     ]
-    ld_small = [load(decay_bias, bias), load(head_gain, hg), load(ffn_gain, fg)]
-    ld_state = load(gla_state.at[:, 0], state)
-    ld_wo = load(w_output, wo)
-    ld_route = [load(router_group, rg), load(router_expert, re), load(expert_ids, ids)]
-    ld_gu = [load(w_gate.at[0], wgu.at[:, 0:ff]), load(w_up.at[0], wgu.at[:, ff : 2 * ff])]
-    ld_wd = load(w_down.at[0], wd)
 
     def ep_copy(phase, src, dst, peer, slot):
         return pltpu.make_async_remote_copy(
@@ -241,6 +233,13 @@
     ld_res.wait()
     pl.semaphore_wait(barrier, n - 1 + t - 1)
     ep_phase_send(0, a_src, a_rx)
+
+    ld_small = [load(decay_bias, bias), load(head_gain, hg), load(ffn_gain, fg)]
+    ld_state = load(gla_state.at[:, 0], state)
+    ld_wo = load(w_output, wo)
+    ld_route = [load(router_group, rg), load(router_expert, re), load(expert_ids, ids)]
+    ld_gu = [load(w_gate.at[0], wgu.at[:, 0:ff]), load(w_up.at[0], wgu.at[:, ff : 2 * ff])]
+    ld_wd = load(w_down.at[0], wd)
     own = res[...]
     a_rx[e] = take_cols(res, e, cols) if aligned else own
     own_float = own.astype(F32)
@@ -275,6 +274,11 @@
     for copy in ld_route + ld_gu:
         copy.wait()
     fg_row[...] = as_row(fg)
+    experts, groups = re.shape[0], rg.shape[0]
+    both[...] = jnp.zeros_like(both)
+    both[0:experts, :] = re[...].astype(F32)
+    both[experts : experts + groups, :] = rg[...].astype(F32)
+    route[...] = both[...].T.astype(BF16)
     b_rx[e] = b_tx[e]
     ep_wait_all(1, b_rx)
     total = jnp.sum(b_rx[...].astype(F32), axis=0) * token_scale
@@ -327,44 +331,44 @@
     tp_wait_all(0, d1_rx)
     attention = jnp.sum(d1_rx[...].astype(F32), axis=0)
     hid = (rows_a[...] + attention).astype(BF16)
+    d2_tx[...] = hid
+    d2_src = lambda peer: d2_tx
+    ep_phase_send(3, d2_src, d2_rx)
     d2_rx[e] = hid
-    d2_src = lambda peer: d2_rx.at[e]
-    ep_phase_send(3, d2_src, d2_rx)
-
-    square = jnp.zeros((tokens, 1), F32)
+
+    square = jnp.zeros((tokens, cols), F32)
     gate_up = jnp.zeros((tokens, 2 * ff), F32)
-    group_logits = jnp.zeros((tokens, rg.shape[0]), F32)
-    expert_logits = jnp.zeros((tokens, re.shape[0]), F32)
+    logits = jnp.zeros((tokens, route.shape[1]), F32)
 
     def moe_chunk(src, carry):
-        square, gate_up, group_logits, expert_logits = carry
+        square, gate_up, logits = carry
         piece = d2_rx[src].astype(F32)
-        square = square + jnp.sum(piece * piece, axis=-1, keepdims=True)
+        square = square + piece * piece
         piece = (piece * take_cols(fg_row, src, cols).astype(F32)).astype(BF16)
         span = pl.ds(pl.multiple_of(src * cols, cols), cols)
         gate_up = gate_up + mm(piece, wgu[span, :])
-        group_logits = group_logits + mm_nt(piece, take_cols(rg, src, cols))
-        expert_logits = expert_logits + mm_nt(piece, take_cols(re, src, cols))
-        return square, gate_up, group_logits, expert_logits
+        logits = logits + mm(piece, route[span, :])
+        return square, gate_up, logits
 
     def moe_step(src, carry):
         ep_wait(3, d2_rx, src)
         return moe_chunk(src, carry)
 
-    carry = moe_chunk(e, (square, gate_up, group_logits, expert_logits))
+    carry = moe_chunk(e, (square, gate_up, logits))
     if n <= 8:
-        for d in range(1, n):
-            carry = moe_step(flip(e, n, d), carry)
+        for part in (range(1, n // 2), range(n // 2, n)):
+            for d in part:
+                ep_wait(3, d2_rx, flip(e, n, d))
+            for d in part:
+                carry = moe_chunk(flip(e, n, d), carry)
     else:
         carry = lax.fori_loop(1, n, lambda d, c: moe_step(lax.rem(e + d, n), c), carry)
-    square, gate_up, group_logits, expert_logits = carry
+    square, gate_up, logits = carry
+    square = jnp.sum(square, axis=-1, keepdims=True)
     scale = lax.rsqrt(square / (n * cols) + EPSILON)
     gate_up = gate_up * scale
-    group_logits = group_logits * scale
-    expert_logits = expert_logits * scale
-
-    groups = group_logits.shape[1]
-    experts = expert_logits.shape[1]
+    logits = logits * scale
+
     diagonal = lax.broadcasted_iota(jnp.int32, (tokens, tokens), 0) == (
         lax.broadcasted_iota(jnp.int32, (tokens, tokens), 1)
     )
@@ -372,13 +376,14 @@
     first, second = column(ids[0:1, :]), column(ids[1:2, :])
     named = (first == e) | (second == e)
     rival = jnp.where(first == e, second, first)
-    expert_at = lax.broadcasted_iota(jnp.int32, expert_logits.shape, 1)
-    group_at = lax.broadcasted_iota(jnp.int32, group_logits.shape, 1)
+    at = lax.broadcasted_iota(jnp.int32, logits.shape, 1)
     pick = lambda mask, values: jnp.sum(jnp.where(mask, values, 0.0), axis=1, keepdims=True)
-    chosen = pick(expert_at == e, expert_logits)
-    rival_logit = pick(expert_at == rival, expert_logits)
-    group_logit = pick(group_at == e // (experts // groups), group_logits)
-    share = 1.0 / jnp.sum(jnp.exp(group_logits - group_logit), axis=1, keepdims=True)
+    chosen = pick(at == e, logits)
+    rival_logit = pick(at == rival, logits)
+    group_logit = pick(at == experts + e // (experts // groups), logits)
+    is_group = (at >= experts) & (at < experts + groups)
+    shifted = jnp.where(is_group, logits - group_logit, 0.0)
+    share = 1.0 / pick(is_group, jnp.exp(shifted))
     weight = jnp.where(named, share / (1.0 + jnp.exp(rival_logit - chosen)), 0.0)
 
     gate, up = gate_up[:, 0:ff], gate_up[:, ff : 2 * ff]
@@ -481,6 +486,7 @@
         w_up,
         w_down,
     )
+    route_cols = -(-(router_expert.shape[0] + router_group.shape[1]) // LANES) * LANES
     dma = pltpu.SemaphoreType.DMA
     scratch = [
         pltpu.VMEM((seqs, width), BF16),
@@ -495,6 +501,8 @@
         pltpu.VMEM((1, width), F32),
         pltpu.VMEM(router_group.shape[::-1], BF16),
         pltpu.VMEM(router_expert.shape, BF16),
+        pltpu.VMEM((route_cols, width), F32),
+        pltpu.VMEM((width, route_cols), BF16),
         pltpu.VMEM(expert_ids.shape[::-1], jnp.int32),
         pltpu.VMEM((width, 2 * ff), BF16),
         pltpu.VMEM((ff, width), BF16),
@@ -506,6 +514,7 @@
         pltpu.VMEM((seqs, vw), BF16),
         pltpu.VMEM((n, seqs, vw), BF16),
         pltpu.VMEM((t, tokens, out_cols), BF16),
+        pltpu.VMEM((tokens, out_cols), BF16),
         pltpu.VMEM((tokens, out_cols), BF16),
         pltpu.VMEM((n, tokens, out_cols), BF16),
         pltpu.VMEM((n, seqs, width), BF16),

time: 36.2 us -> 35.9 us (level)
  no operation moved by 1% of the time
where the time goes in v3:
time: 35.9 us; the launch traced here: 35.7 us
  Pallas kernels  33.5 us (93%)
  local copies, waits for them, and re-layouts  1.57 us (4%)
  between operations  0.65 us (2%)
    pallas_call x1, Pallas kernels, on_device(): pl.pallas_call(functools.partial(kernel, n, t), out_shape=(jax.ShapeDtype...  33.5 us
    unnamed x2, local copies, waits for them, and re-layouts  1.57 us

profile of v3, /device:TPU:0, one launch (start us, length us, event | category | flops | bytes accessed | tf_op | source)
XLA Modules:
  0.0 35.7 jit_solution(6390282071023823861)
XLA Ops:
  0.6 33.5 %shard_map.176 = (bf16[2,2048]{1,0:T(2,128)(2,1)S(1)}, f32[2,1,256,512]{3,2,1,0:T(8,128)S(1)}) custom-call(bf16[2,2048]{1,0:T(2,128)(2,1)} %residual_in.1, f32[2,1,256,512]{3,2,1,0:T(8,128)} %gla_state.1, bf16[16,128]{1,0:T(8,128)(2,1)} %bitcast.7, bf16[256,256]{1,0:T(8,128)(2,1)} %w_query.1, bf16[256,256]{1,0:T(8,128)(2,1)} %w_key.1, ...), custom_call_target="tpu_custom_call" | custom-call | tf_op jit(solution)/shard_map/pallas_call | solution.py:536
  34.1 0.6 %copy.21 = bf16[2,2048]{1,0:T(2,128)(2,1)} copy(bf16[2,2048]{1,0:T(2,128)(2,1)S(1)} %get-tuple-element.4) | data formatting | bytes 16384
  34.7 1.0 %copy.22 = f32[2,1,256,512]{3,2,1,0:T(8,128)} copy(f32[2,1,256,512]{3,2,1,0:T(8,128)S(1)} %get-tuple-element.5) | data formatting | bytes 2097152
